TPU v7x, 32 devices: a whole 2x2x4 slice. The times are simulated.
32 devices in a mesh: fs: 8 (over z, x), tp: 4 (over y, core).
Axes of the slice: x: 2, y: 2, z: 4, core: 2. Of those that a mesh axis runs over, the one named last changes fastest.
Arguments:
- saved_input: bfloat16 [24576, 2048], P('fs'), may hold values from -6 to 6
- proj_cot: bfloat16 [3, 24576, 2048], P(None, 'fs', 'tp'), may hold values from -0.0390625 to 0.0390625
- log_cache: float32 [16, 24576], P(None, 'fs'), as said below
- cache_cot: float32 [16, 24576], P(None, 'fs'), may hold values from -0.0390625 to 0.0390625
- proj_master: float32 [3, 2048, 2048], P(None, 'fs', 'tp'), may hold values from -0.125 to 0.125
- factors: bfloat16 [3, 2048, 256], P(None, 'fs'), may hold values from -0.125 to 0.125
- first_moment: float32 [3, 256, 2048], P(None, None, 'tp'), may hold values from -6 to 6
- second_moment: float32 [3, 256, 2048], P(None, None, 'tp'), may hold values from 0.01 to 10
- gate_master: float32 [16, 2048], replicated, may hold values from -0.125 to 0.125
- gate_first: float32 [16, 2048], replicated, may hold values from -6 to 6
- gate_second: float32 [16, 2048], replicated, may hold values from 0.1 to 3
Outputs:
- proj_step: float32 [3, 2048, 2048], P(None, 'fs', 'tp')
- proj_new: float32 [3, 2048, 2048], P(None, 'fs', 'tp')
- proj_copy: bfloat16 [3, 2048, 2048], P(None, None, 'tp')
- first_new: float32 [3, 256, 2048], P(None, None, 'tp')
- second_new: float32 [3, 256, 2048], P(None, None, 'tp')
- gate_new: float32 [16, 2048], replicated
- gate_copy: bfloat16 [16, 2048], replicated
- gate_first_new: float32 [16, 2048], replicated
- gate_second_new: float32 [16, 2048], replicated
Inputs may be any that keep to these rules, and one draw needn't show every extreme that they name: `log_cache`: each head's values never rise along positions.
All inputs are finite; a program needn't handle non-finite values.
Results may differ from a plain program's by a relative error of at most 0.0004.
Values may be sent and summed in bfloat16 or wider, within the bound.
A program may use at most 128 MiB of HBM per device.

v0:
```python
import jax
import jax.numpy as jnp
from jax import lax
from jax.sharding import PartitionSpec as P

BETA_ONE = 0.8
BETA_TWO = 0.9
LEARN = 0.001


def from_behind(x, axis, by):
    peers = lax.axis_size(axis)
    pairs = [(i, i + by) for i in range(peers) if 0 <= i + by < peers]
    return lax.ppermute(x, axis, pairs)


def prefix(value, axis, join, neutral):
    count, mine = (lax.axis_size(axis), lax.axis_index(axis))
    pieces = lax.all_gather(value, axis)
    pieces = pieces[::-1]
    mine = count - 1 - mine
    so_far = jnp.full_like(value, 0) + jnp.asarray(neutral, value.dtype)

    def hop(position, so_far):
        longer = join(so_far, pieces[position])
        return jnp.where(position < mine, longer, so_far)

    return lax.fori_loop(0, count - 1, hop, so_far)


def add_pair(earlier, later_part):
    return earlier + later_part


def local(
    saved_input,
    proj_cot,
    log_cache,
    cache_cot,
    proj_master,
    factors,
    first_moment,
    second_moment,
    gate_master,
    gate_first,
    gate_second,
):
    heads = log_cache.shape[0]
    edge = from_behind(log_cache[:, -1:], "fs", 1)
    previous = jnp.concatenate([edge, log_cache[:, :-1]], axis=1)
    gate_logarithm = log_cache - previous
    carried = prefix(jnp.sum(cache_cot, axis=1), "fs", add_pair, jnp.zeros((heads,), jnp.float32))
    later = jnp.flip(jnp.cumsum(jnp.flip(cache_cot, 1), axis=1), 1) + carried[:, None]
    gate_cot = (later * -jnp.expm1(gate_logarithm)).astype(jnp.bfloat16)
    gate_part = jnp.dot(gate_cot, saved_input, preferred_element_type=jnp.float32)
    all_factors = lax.all_gather(factors, "fs", axis=1, tiled=True)
    reduced = jnp.einsum(
        "td,rdk->rtk", saved_input, all_factors, preferred_element_type=jnp.float32
    )
    upper_half = lax.optimization_barrier(reduced.astype(jnp.bfloat16))
    lower_half = (reduced - upper_half.astype(jnp.float32)).astype(jnp.bfloat16)
    low_part = jnp.einsum("rtk,rtw->rkw", upper_half, proj_cot, preferred_element_type=jnp.float32)
    low_part = low_part + jnp.einsum(
        "rtk,rtw->rkw", lower_half, proj_cot, preferred_element_type=jnp.float32
    )
    low, gate_grad = lax.psum((low_part, gate_part), "fs")
    first_new = BETA_ONE * first_moment + (1.0 - BETA_ONE) * low
    second_new = BETA_TWO * second_moment + (1.0 - BETA_TWO) * low * low
    direction = first_new / jnp.sqrt(second_new)
    squares = lax.psum(jnp.sum(direction * direction), "tp")
    entries = direction.shape[0] * direction.shape[1] * direction.shape[2] * lax.axis_size("tp")
    scale = lax.rsqrt(squares / entries + 1e-06)
    product = jnp.einsum(
        "rdk,rkw->rdw", factors.astype(jnp.float32), direction, precision=lax.Precision.HIGHEST
    )
    proj_step = scale * product
    proj_new = proj_master - LEARN * proj_step
    proj_copy = lax.all_gather(proj_new.astype(jnp.bfloat16), "fs", axis=1, tiled=True)
    gate_first_new = BETA_ONE * gate_first + (1.0 - BETA_ONE) * gate_grad
    gate_second_new = BETA_TWO * gate_second + (1.0 - BETA_TWO) * gate_grad * gate_grad
    gate_new = gate_master - LEARN * gate_first_new / jnp.sqrt(gate_second_new)
    gate_copy = gate_new.astype(jnp.bfloat16)
    return (
        proj_step,
        proj_new,
        proj_copy,
        first_new,
        second_new,
        gate_new,
        gate_copy,
        gate_first_new,
        gate_second_new,
    )


def solution(mesh):
    placed = (
        P("fs", None),
        P(None, "fs", "tp"),
        P(None, "fs"),
        P(None, "fs"),
        P(None, "fs", "tp"),
        P(None, "fs", None),
        P(None, None, "tp"),
        P(None, None, "tp"),
        P(),
        P(),
        P(),
    )
    return jax.shard_map(
        local,
        mesh=mesh,
        in_specs=placed,
        out_specs=(
            P(None, "fs", "tp"),
            P(None, "fs", "tp"),
            P(None, None, "tp"),
            P(None, None, "tp"),
            P(None, None, "tp"),
            P(),
            P(),
            P(),
            P(),
        ),
        check_vma=False,
    )
```

profile of v0, /device:TPU:0, one launch (start us, length us, event | category | flops | bytes accessed | tf_op | source)
XLA Modules:
  0.0 330.7 jit_solution(11614293912108282255)
XLA Ops:
  7.2 2.0 copy.26
  9.3 0.8 slice.14
  10.1 4.9 %collective-permute-start = (f32[16,1]{1,0:T(8,128)S(1)}, f32[16,1]{1,0:T(8,128)S(1)}, u32[]{:S(2)}, u32[]{:S(2)}) collective-permute-start(f32[16,1]{1,0:T(8,128)S(1)} %slice.14), channel_id=1, source_target_pairs={{0,4},{4,8},{8,12},{12,16},{16,20},{20,24},{24,28},{1,5},{5,9},{9,... | collective-permute-start | bytes 200 | tf_op jit(solution)/shard_map/ppermute | solution.py:14
  15.0 9.3 %rev.10 = f32[16,3072]{1,0:T(8,128)S(1)} reverse(f32[16,3072]{1,0:T(8,128)} %param.16), dimensions={1} | reverse | bytes 393216 | tf_op jit(solution)/shard_map/jit(_flip)/rev | solution.py:53
  24.5 4.6 %reduce-window.6 = f32[16,24,128]{2,1,0:T(8,128)S(1)} reduce-window(f32[16,24,128]{2,1,0:T(8,128)S(1)} %bitcast.36, f32[]{:T(128)} %constant.50.clone.1), window={size=1x1x128 pad=0_0x0_0x127_0}, to_apply=%region_3.4 | reduce-window | flops 6242304 | bytes 393220 | tf_op jit(solution)/shard_map/reduce-window
  29.7 0.6 dynamic-slice
  31.2 19.9 %all-reduce = f32[128]{0:T(128)S(1)} all-reduce(f32[128]{0:T(128)S(1)} %dynamic-update-slice), channel_id=2, replica_groups=mesh['fs'=8,'tp'=4] {'fs'}, use_global_device_ids=true, to_apply=%add | all-reduce | flops 128 | bytes 1024
  51.4 1.7 rev.11
  53.2 7.1 %fusion.14 = f32[16,2048]{1,0:T(8,128)} fusion(bf16[3072,2048]{1,0:T(8,128)(2,1)} %param.13, f32[16,3072]{1,0:T(8,128)S(1)} %copy-done.2, f32[16,3071]{1,0:T(8,128)S(1)} %bitcast.34, f32[16,1]{1,0:T(8,128)S(1)} %collective-permute-done, f32[16,3072]{1,0:T(8,128)S(1)} %rev.11, f32[16]{0:T(128)S(1)} %get-tuple-element.88), kind=kOutput, calls=%fused_computation.27 | convolution fusion | flops 201621504 | bytes 13303872 | tf_op jit(solution)/shard_map/dot_general | solution.py:55
  60.3 15.9 %all-gather.4.cloned.1.call-done = bf16[3,2048,256]{1,2,0:T(8,128)(2,1)} async-done(((bf16[3,256,256]{1,2,0:T(8,128)(2,1)}), bf16[3,2048,256]{1,2,0:T(8,128)(2,1)}) %all-gather.4.cloned.1.call-update) | async-done | bytes 3145744 | tf_op jit(solution)/shard_map/all_gather | solution.py:56
  76.1 16.1 %bitcast_convert_fusion = (bf16[3,3072,256]{1,2,0:T(8,128)(2,1)S(1)}, f32[3,256,3072]{2,1,0:T(8,128)}) fusion(bf16[3,2048,256]{1,2,0:T(8,128)(2,1)} %all-gather.4.cloned.1.call-done, bf16[3072,2048]{1,0:T(8,128)(2,1)} %param.13), kind=kOutput, calls=%fused_computation.5 | convolution fusion | flops 9666035712 | bytes 29884416 | tf_op jit(solution)/shard_map/td,rdk->rtk/dot_general | solution.py:57
  92.2 5.3 %fusion.22 = f32[3,256,512]{2,1,0:T(8,128)S(1)} fusion(bf16[3,3072,256]{1,2,0:T(8,128)(2,1)S(1)} %get-tuple-element.141, bf16[3,3072,512]{2,1,0:T(8,128)(2,1)} %param.14), kind=kOutput, calls=%fused_computation.33 | convolution fusion | flops 2415919104 | bytes 15728640 | tf_op jit(solution)/shard_map/rtk,rtw->rkw/dot_general | solution.py:62
  97.6 10.2 %fusion.6 = f32[3,256,512]{2,1,0:T(8,128)} fusion(f32[3,256,512]{2,1,0:T(8,128)S(1)} %fusion.22, bf16[3,3072,512]{2,1,0:T(8,128)(2,1)} %param.14, f32[3,256,3072]{2,1,0:T(8,128)} %get-tuple-element.142, bf16[3,3072,256]{1,2,0:T(8,128)(2,1)S(1)} %get-tuple-element.141), kind=kOutput, calls=%fused_computation.15 | convolution fusion | flops 2423390208 | bytes 26738688 | tf_op jit(solution)/shard_map/rtk,rtw->rkw/dot_general | solution.py:63
  107.9 1.3 copy-done.1
  109.2 0.5 copy.28
  109.7 89.2 %all-reduce.4.cloned.1.call-done = (f32[3,256,512]{2,1,0:T(8,128)}, f32[16,2048]{1,0:T(8,128)}) async-done(((f32[3,256,512]{2,1,0:T(8,128)}, f32[16,2048]{1,0:T(8,128)}), (f32[3,256,512]{2,1,0:T(8,128)}, f32[16,2048]{1,0:T(8,128)})) %all-reduce.4.cloned.1.call-update) | async-done | bytes 1703952 | tf_op jit(solution)/shard_map/psum | solution.py:66
  198.9 5.5 %multiply_reduce_fusion = (f32[]{:T(128)}, f32[3,256,512]{2,1,0:T(8,128)}, f32[3,256,512]{2,1,0:T(8,128)}) fusion(f32[3,256,512]{2,1,0:T(8,128)} %get-tuple-element.130, f32[3,256,512]{2,1,0:T(8,128)} %param.20, f32[3,256,512]{2,1,0:T(8,128)} %param.19), kind=kLoop, calls=%fused_computation.12 | loop fusion | flops 3932159 | bytes 7864324 | tf_op jit(solution)/shard_map/reduce_sum | solution.py:70
  204.4 7.6 %psum.22 = f32[]{:T(128)} all-reduce(f32[]{:T(128)} %get-tuple-element.138), channel_id=1, replica_groups=mesh['fs'=8,'tp'=4] {'tp'}, use_global_device_ids=true, to_apply=%region_2.3 | all-reduce | flops 1 | bytes 8 | tf_op jit(solution)/shard_map/psum | solution.py:70
  212.7 4.8 %fusion.20 = (bf16[3,256,512]{1,2,0:T(8,128)(2,1)}, f32[3,256,512]{1,2,0:T(8,128)S(1)}, f32[3,256,512]{1,2,0:T(8,128)}) fusion(f32[3,256,512]{1,2,0:T(8,128)S(1)} %copy.28, bf16[3,256,256]{2,1,0:T(8,128)(2,1)S(1)} %copy-done, f32[3,256,512]{2,1,0:T(8,128)} %get-tuple-element.140, f32[3,256,512]{2,1,0:T(8,128)} %get-tuple-element.139, f32[]{:T(128)S(6)} %rsqrt.5), kind=kOutput, calls=%fused_computation.32 | convolution fusion | flops 1209925632 | bytes 9043972 | tf_op jit(solution)/shard_map/rdk,rkw->rdw/dot_general | solution.py:73
  217.5 3.0 copy.29
  220.6 1.6 copy.30
  222.2 0.8 fusion.18
  223.0 92.6 %all-gather.6.cloned.1.call-done = bf16[3,2048,512]{1,2,0:T(8,128)(2,1)} async-done(((bf16[3,256,512]{1,2,0:T(8,128)(2,1)}), bf16[3,2048,512]{1,2,0:T(8,128)(2,1)}) %all-gather.6.cloned.1.call-update) | async-done | bytes 6291472 | tf_op jit(solution)/shard_map/all_gather | solution.py:78
  315.6 8.6 %copy.31 = bf16[3,2048,512]{2,1,0:T(8,128)(2,1)} copy(bf16[3,2048,512]{1,2,0:T(8,128)(2,1)} %all-gather.6.cloned.1.call-done) | data formatting | bytes 12582912
  (43 shorter events, 1.7 us)
Async XLA Ops:
  7.2 17.2 %copy-start.3 = (f32[16,3072]{1,0:T(8,128)S(1)}, f32[16,3072]{1,0:T(8,128)}, u32[]{:S(2)}) copy-start(f32[16,3072]{1,0:T(8,128)} %param.16) | copy-start | bytes 589828
  7.2 68.9 %all-gather.4.cloned.1.call-start = ((), (), s32[]{:S(2)}) async-start(), calls=%async_computation | async-start | bytes 3538944 | tf_op jit(solution)/shard_map/all_gather | solution.py:56
  9.2 20.5 %copy-start.8 = (u32[32]{0:T(128)S(1)}, u32[32]{0:T(128)}, u32[]{:S(2)}) copy-start(u32[32]{0:T(128)} %constant.60) | copy-start | bytes 388
  9.2 43.9 %copy-start.2 = (f32[16,3072]{1,0:T(8,128)S(1)}, f32[16,3072]{1,0:T(8,128)}, u32[]{:S(2)}) copy-start(f32[16,3072]{1,0:T(8,128)} %param.15) | copy-start | bytes 589828
  9.2 189.7 %all-reduce.4.cloned.1.call-start = ((), (), s32[]{:S(2)}) async-start(), calls=%async_computation.2 | async-start | bytes 3407872 | tf_op jit(solution)/shard_map/psum | solution.py:66
  10.1 43.1 %collective-permute-start = (f32[16,1]{1,0:T(8,128)S(1)}, f32[16,1]{1,0:T(8,128)S(1)}, u32[]{:S(2)}, u32[]{:S(2)}) collective-permute-start(f32[16,1]{1,0:T(8,128)S(1)} %slice.14), channel_id=1, source_target_pairs={{0,4},{4,8},{8,12},{12,16},{16,20},{20,24},{24,28},{1,5},{5,9},{9,... | collective-permute-start | bytes 200 | tf_op jit(solution)/shard_map/ppermute | solution.py:14
  107.8 1.4 copy-start.1
  107.8 207.7 %all-gather.6.cloned.1.call-start = ((), (), s32[]{:S(2)}) async-start(), calls=%async_computation.1 | async-start | bytes 7077888 | tf_op jit(solution)/shard_map/all_gather | solution.py:78
  198.9 13.8 %copy-start = (bf16[3,256,256]{2,1,0:T(8,128)(2,1)S(1)}, bf16[3,256,256]{2,1,0:T(8,128)(2,1)}, u32[]{:S(2)}) copy-start(bf16[3,256,256]{2,1,0:T(8,128)(2,1)} %param.18) | copy-start | bytes 1179652
  220.6 1.6 copy-start.4
  220.6 1.6 copy-start.5
  220.6 1.6 copy-start.6
  220.6 1.6 copy-start.7
Sparse Core Ops, SparseCore 0:
  10.6 65.4 all-gather.3
  107.9 90.9 all-reduce.3
  217.7 97.8 all-gather.5
where the time goes:
time: 332 us; the launch traced here: 331 us
  waiting for transfers between devices  198 us (60%)
  matrix products  43.6 us (13%)
  local copies, waits for them, and re-layouts  30.1 us (9%)
  blocking collectives  27.5 us (8%)
  between operations  15.3 us (5%)
  other arithmetic  11.4 us (3%)
  starting transfers between devices  4.98 us (2%)
    all_gather x1, waiting for transfers between devices, local(): lax.all_gather(proj_new.astype(jnp.bfloat16), 'fs', axis=1, tiled=True)  92.6 us
    psum x1, waiting for transfers between devices, local(): low, gate_grad = lax.psum((low_part, gate_part), 'fs')  89.2 us
    unnamed x1, blocking collectives  19.9 us
    unnamed x28, local copies, waits for them, and re-layouts  17.9 us
    dot_general x1, matrix products, local(): jnp.einsum('td,rdk->rtk', saved_input, all_factors, preferred_element_typ...  16.1 us
    all_gather x1, waiting for transfers between devices, local(): all_factors = lax.all_gather(factors, 'fs', axis=1, tiled=True)  15.9 us
    dot_general x1, matrix products, local(): jnp.einsum('rtk,rtw->rkw', lower_half, proj_cot, preferred_element_type=j...  10.2 us
    rev x1, local copies, waits for them, and re-layouts, local(): jnp.flip(cache_cot, 1)  9.35 us
  transfers between devices with their start and end apart: 4, of which 3 were waited for; matrix products, arithmetic and copies ran while one was open for 9% of the time, Pallas kernels for 0%

commit v1 on v0

--- a/solution.py
+++ b/solution.py
@@ -75,7 +75,12 @@
     )
     proj_step = scale * product
     proj_new = proj_master - LEARN * proj_step
-    proj_copy = lax.all_gather(proj_new.astype(jnp.bfloat16), "fs", axis=1, tiled=True)
+    proj_copy = jnp.concatenate(
+        lax.all_to_all(
+            jnp.stack([proj_new.astype(jnp.bfloat16)] * lax.axis_size("fs")), "fs", 0, 0
+        ),
+        axis=1,
+    )
     gate_first_new = BETA_ONE * gate_first + (1.0 - BETA_ONE) * gate_grad
     gate_second_new = BETA_TWO * gate_second + (1.0 - BETA_TWO) * gate_grad * gate_grad
     gate_new = gate_master - LEARN * gate_first_new / jnp.sqrt(gate_second_new)

time: 332 us -> 378 us (1.14)
  waiting for transfers between devices: 198 us -> 238 us
  starting transfers between devices: 4.98 us -> 9.83 us
    all_to_all x0 -> x1, waiting for transfers between devices: none -> 133 us  [local(): lax.all_to_all(jnp.stack([proj_new.astype(jnp.bfloat16)] * lax.axis_size(...]
    all_gather x1 -> x0, waiting for transfers between devices: 92.6 us -> none  [local(): lax.all_gather(proj_new.astype(jnp.bfloat16), 'fs', axis=1, tiled=True)]
    unnamed x28 -> x29, local copies, waits for them, and re-layouts: 17.9 us -> 7.97 us
    all_to_all x0 -> x1, local copies, waits for them, and re-layouts: none -> 6.09 us  [local(): lax.all_to_all(jnp.stack([proj_new.astype(jnp.bfloat16)] * lax.axis_size(...]
    all_to_all x0 -> x1, starting transfers between devices: none -> 4.89 us  [local(): lax.all_to_all(jnp.stack([proj_new.astype(jnp.bfloat16)] * lax.axis_size(...]
  transfers between devices with their start and end apart: 4 -> 4, of which waited for: 3 -> 3; matrix products, arithmetic and copies ran while one was open for 9% -> 8% of each run, Pallas kernels for 0% -> 0%
where the time goes in v1:
time: 378 us; the launch traced here: 377 us
  waiting for transfers between devices  238 us (63%)
  matrix products  43.6 us (12%)
  local copies, waits for them, and re-layouts  31.1 us (8%)
  blocking collectives  27.5 us (7%)
  between operations  15.6 us (4%)
  other arithmetic  11.4 us (3%)
  starting transfers between devices  9.83 us (3%)
    all_to_all x1, waiting for transfers between devices, local(): lax.all_to_all(jnp.stack([proj_new.astype(jnp.bfloat16)] * lax.axis_size(...  133 us
    psum x1, waiting for transfers between devices, local(): low, gate_grad = lax.psum((low_part, gate_part), 'fs')  89.2 us
    unnamed x1, blocking collectives  19.9 us
    dot_general x1, matrix products, local(): jnp.einsum('td,rdk->rtk', saved_input, all_factors, preferred_element_typ...  16.1 us
    all_gather x1, waiting for transfers between devices, local(): all_factors = lax.all_gather(factors, 'fs', axis=1, tiled=True)  15.9 us
    dot_general x1, matrix products, local(): jnp.einsum('rtk,rtw->rkw', lower_half, proj_cot, preferred_element_type=j...  10.2 us
    rev x1, local copies, waits for them, and re-layouts, local(): jnp.flip(cache_cot, 1)  9.35 us
    unnamed x29, local copies, waits for them, and re-layouts  7.97 us
  transfers between devices with their start and end apart: 4, of which 3 were waited for; matrix products, arithmetic and copies ran while one was open for 8% of the time, Pallas kernels for 0%

profile of v1, /device:TPU:0, one launch (start us, length us, event | category | flops | bytes accessed | tf_op | source)
XLA Modules:
  0.0 377.4 jit_solution(8041268441333437275)
XLA Ops:
  7.2 2.0 copy.38
  9.3 0.8 slice.14
  10.1 4.9 %collective-permute-start = (f32[16,1]{1,0:T(8,128)S(1)}, f32[16,1]{1,0:T(8,128)S(1)}, u32[]{:S(2)}, u32[]{:S(2)}) collective-permute-start(f32[16,1]{1,0:T(8,128)S(1)} %slice.14), channel_id=1, source_target_pairs={{0,4},{4,8},{8,12},{12,16},{16,20},{20,24},{24,28},{1,5},{5,9},{9,... | collective-permute-start | bytes 200 | tf_op jit(solution)/shard_map/ppermute | solution.py:14
  15.0 9.3 %rev.10 = f32[16,3072]{1,0:T(8,128)S(1)} reverse(f32[16,3072]{1,0:T(8,128)} %param.16), dimensions={1} | reverse | bytes 393216 | tf_op jit(solution)/shard_map/jit(_flip)/rev | solution.py:53
  24.5 4.6 %reduce-window.6 = f32[16,24,128]{2,1,0:T(8,128)S(1)} reduce-window(f32[16,24,128]{2,1,0:T(8,128)S(1)} %bitcast.40, f32[]{:T(128)} %constant.50.clone.1), window={size=1x1x128 pad=0_0x0_0x127_0}, to_apply=%region_3.4 | reduce-window | flops 6242304 | bytes 393220 | tf_op jit(solution)/shard_map/reduce-window
  31.2 19.9 %all-reduce = f32[128]{0:T(128)S(1)} all-reduce(f32[128]{0:T(128)S(1)} %dynamic-update-slice), channel_id=2, replica_groups=mesh['fs'=8,'tp'=4] {'fs'}, use_global_device_ids=true, to_apply=%add | all-reduce | flops 128 | bytes 1024
  51.4 1.7 rev.11
  53.2 7.1 %fusion.14 = f32[16,2048]{1,0:T(8,128)} fusion(bf16[3072,2048]{1,0:T(8,128)(2,1)} %param.13, f32[16,3072]{1,0:T(8,128)S(1)} %copy-done.3, f32[16,3071]{1,0:T(8,128)S(1)} %bitcast.38, f32[16,1]{1,0:T(8,128)S(1)} %collective-permute-done, f32[16,3072]{1,0:T(8,128)S(1)} %rev.11, f32[16]{0:T(128)S(1)} %get-tuple-element.88), kind=kOutput, calls=%fused_computation.27 | convolution fusion | flops 201621504 | bytes 13303872 | tf_op jit(solution)/shard_map/dot_general | solution.py:55
  60.3 15.9 %all-gather.3.cloned.1.call-done = bf16[3,2048,256]{1,2,0:T(8,128)(2,1)} async-done(((bf16[3,256,256]{1,2,0:T(8,128)(2,1)}), bf16[3,2048,256]{1,2,0:T(8,128)(2,1)}) %all-gather.3.cloned.1.call-update) | async-done | bytes 3145744 | tf_op jit(solution)/shard_map/all_gather | solution.py:56
  76.1 16.1 %bitcast_convert_fusion = (bf16[3,3072,256]{1,2,0:T(8,128)(2,1)S(1)}, f32[3,256,3072]{2,1,0:T(8,128)}) fusion(bf16[3,2048,256]{1,2,0:T(8,128)(2,1)} %all-gather.3.cloned.1.call-done, bf16[3072,2048]{1,0:T(8,128)(2,1)} %param.13), kind=kOutput, calls=%fused_computation.5 | convolution fusion | flops 9666035712 | bytes 29884416 | tf_op jit(solution)/shard_map/td,rdk->rtk/dot_general | solution.py:57
  92.2 5.3 %fusion.22 = f32[3,256,512]{2,1,0:T(8,128)S(1)} fusion(bf16[3,3072,256]{1,2,0:T(8,128)(2,1)S(1)} %get-tuple-element.159, bf16[3,3072,512]{2,1,0:T(8,128)(2,1)} %param.14), kind=kOutput, calls=%fused_computation.33 | convolution fusion | flops 2415919104 | bytes 15728640 | tf_op jit(solution)/shard_map/rtk,rtw->rkw/dot_general | solution.py:62
  97.6 10.2 %fusion.6 = f32[3,256,512]{2,1,0:T(8,128)} fusion(f32[3,256,512]{2,1,0:T(8,128)S(1)} %fusion.22, bf16[3,3072,512]{2,1,0:T(8,128)(2,1)} %param.14, f32[3,256,3072]{2,1,0:T(8,128)} %get-tuple-element.160, bf16[3,3072,256]{1,2,0:T(8,128)(2,1)S(1)} %get-tuple-element.159), kind=kOutput, calls=%fused_computation.15 | convolution fusion | flops 2423390208 | bytes 26738688 | tf_op jit(solution)/shard_map/rtk,rtw->rkw/dot_general | solution.py:63
  107.8 1.4 copy-done.2
  109.7 89.2 %all-reduce.4.cloned.1.call-done = (f32[3,256,512]{2,1,0:T(8,128)}, f32[16,2048]{1,0:T(8,128)}) async-done(((f32[3,256,512]{2,1,0:T(8,128)}, f32[16,2048]{1,0:T(8,128)}), (f32[3,256,512]{2,1,0:T(8,128)}, f32[16,2048]{1,0:T(8,128)})) %all-reduce.4.cloned.1.call-update) | async-done | bytes 1703952 | tf_op jit(solution)/shard_map/psum | solution.py:66
  198.9 5.5 %multiply_reduce_fusion = (f32[]{:T(128)}, f32[3,256,512]{2,1,0:T(8,128)}, f32[3,256,512]{2,1,0:T(8,128)}) fusion(f32[3,256,512]{2,1,0:T(8,128)} %get-tuple-element.148, f32[3,256,512]{2,1,0:T(8,128)} %param.20, f32[3,256,512]{2,1,0:T(8,128)} %param.19), kind=kLoop, calls=%fused_computation.12 | loop fusion | flops 3932159 | bytes 7864324 | tf_op jit(solution)/shard_map/reduce_sum | solution.py:70
  204.4 7.6 %psum.22 = f32[]{:T(128)} all-reduce(f32[]{:T(128)} %get-tuple-element.156), channel_id=1, replica_groups=mesh['fs'=8,'tp'=4] {'tp'}, use_global_device_ids=true, to_apply=%region_2.3 | all-reduce | flops 1 | bytes 8 | tf_op jit(solution)/shard_map/psum | solution.py:70
  212.7 4.8 %fusion.20 = (bf16[3,256,512]{1,2,0:T(8,128)(2,1)}, f32[3,256,512]{1,2,0:T(8,128)S(1)}, f32[3,256,512]{1,2,0:T(8,128)}) fusion(f32[3,256,512]{1,2,0:T(8,128)S(1)} %copy.40, bf16[3,256,256]{2,1,0:T(8,128)(2,1)S(1)} %copy-done.1, f32[3,256,512]{2,1,0:T(8,128)} %get-tuple-element.158, f32[3,256,512]{2,1,0:T(8,128)} %get-tuple-element.157, f32[]{:T(128)S(6)} %rsqrt.5), kind=kOutput, calls=%fused_computation.32 | convolution fusion | flops 1209925632 | bytes 9043972 | tf_op jit(solution)/shard_map/rdk,rkw->rdw/dot_general | solution.py:73
  217.5 1.4 copy.41
  218.9 3.4 stack.2
  222.3 4.9 %all-to-all-start = ((bf16[8,3,256,512]{3,2,1,0:T(8,128)(2,1)}), bf16[8,3,256,512]{3,2,1,0:T(8,128)(2,1)}, u32[]{:S(2)}, u32[]{:S(2)}) async-start(bf16[8,3,256,512]{3,2,1,0:T(8,128)(2,1)} %stack.2), calls=%async_computation | async-start | bytes 12582912 | tf_op jit(solution)/shard_map/all_to_all | solution.py:79
  227.2 1.6 copy.43
  228.8 1.6 copy.44
  231.2 133.2 %all-to-all-done = bf16[8,3,256,512]{3,2,1,0:T(8,128)(2,1)} async-done(((bf16[8,3,256,512]{3,2,1,0:T(8,128)(2,1)}), bf16[8,3,256,512]{3,2,1,0:T(8,128)(2,1)}, u32[]{:S(2)}, u32[]{:S(2)}) %all-to-all-start) | async-done | bytes 6291488 | tf_op jit(solution)/shard_map/all_to_all | solution.py:79
  364.4 6.1 %copy.42 = bf16[8,3,256,512]{3,2,0,1:T(8,128)(2,1)} copy(bf16[8,3,256,512]{3,2,1,0:T(8,128)(2,1)} %all-to-all-done) | data formatting | bytes 12582912 | tf_op jit(solution)/shard_map/all_to_all | solution.py:79
  (46 shorter events, 3.4 us)
Async XLA Ops:
  7.2 17.2 %copy-start.4 = (f32[16,3072]{1,0:T(8,128)S(1)}, f32[16,3072]{1,0:T(8,128)}, u32[]{:S(2)}) copy-start(f32[16,3072]{1,0:T(8,128)} %param.16) | copy-start | bytes 589828
  7.2 68.9 %all-gather.3.cloned.1.call-start = ((), (), s32[]{:S(2)}) async-start(), calls=%async_computation.1 | async-start | bytes 3538944 | tf_op jit(solution)/shard_map/all_gather | solution.py:56
  9.2 20.5 %copy-start.9 = (u32[32]{0:T(128)S(1)}, u32[32]{0:T(128)}, u32[]{:S(2)}) copy-start(u32[32]{0:T(128)} %constant.60) | copy-start | bytes 388
  9.2 43.9 %copy-start.3 = (f32[16,3072]{1,0:T(8,128)S(1)}, f32[16,3072]{1,0:T(8,128)}, u32[]{:S(2)}) copy-start(f32[16,3072]{1,0:T(8,128)} %param.15) | copy-start | bytes 589828
  9.2 189.7 %all-reduce.4.cloned.1.call-start = ((), (), s32[]{:S(2)}) async-start(), calls=%async_computation.2 | async-start | bytes 3407872 | tf_op jit(solution)/shard_map/psum | solution.py:66
  10.1 43.1 %collective-permute-start = (f32[16,1]{1,0:T(8,128)S(1)}, f32[16,1]{1,0:T(8,128)S(1)}, u32[]{:S(2)}, u32[]{:S(2)}) collective-permute-start(f32[16,1]{1,0:T(8,128)S(1)} %slice.14), channel_id=1, source_target_pairs={{0,4},{4,8},{8,12},{12,16},{16,20},{20,24},{24,28},{1,5},{5,9},{9,... | collective-permute-start | bytes 200 | tf_op jit(solution)/shard_map/ppermute | solution.py:14
  107.8 1.4 copy-start.2
  198.9 13.8 %copy-start.1 = (bf16[3,256,256]{2,1,0:T(8,128)(2,1)S(1)}, bf16[3,256,256]{2,1,0:T(8,128)(2,1)}, u32[]{:S(2)}) copy-start(bf16[3,256,256]{2,1,0:T(8,128)(2,1)} %param.18) | copy-start | bytes 1179652
  222.3 4.9 %copy-start = (f32[3,256,512]{1,2,0:T(8,128)S(1)}, f32[3,256,512]{1,2,0:T(8,128)}, u32[]{:S(2)}) copy-start(f32[3,256,512]{1,2,0:T(8,128)} %get-tuple-element.161) | copy-start | bytes 4718596
  222.3 142.1 %all-to-all-start = ((bf16[8,3,256,512]{3,2,1,0:T(8,128)(2,1)}), bf16[8,3,256,512]{3,2,1,0:T(8,128)(2,1)}, u32[]{:S(2)}, u32[]{:S(2)}) async-start(bf16[8,3,256,512]{3,2,1,0:T(8,128)(2,1)} %stack.2), calls=%async_computation | async-start | bytes 12582912 | tf_op jit(solution)/shard_map/all_to_all | solution.py:79
  228.8 1.6 copy-start.5
  228.8 1.6 copy-start.6
  228.8 1.6 copy-start.7
  228.8 1.6 copy-start.8
Sparse Core Ops, SparseCore 0:
  10.6 65.4 all-gather.2
  107.9 90.9 all-reduce.3
